TPU v7x, 32 devices: a whole 2x2x4 slice. The times are simulated.
32 devices in a mesh: sp: 8 (over z, x), tp: 4 (over y, core).
Axes of the slice: x: 2, y: 2, z: 4, core: 2. Of those that a mesh axis runs over, the one named last changes fastest.
Arguments:
- broad_probe_tensor: bfloat16 [4096, 1024], P('sp', 'tp'), may hold values from -6 to 6
- broad_lookup_tensor: bfloat16 [4096, 1024], P('sp', 'tp'), may hold values from -6 to 6
- broad_payload_tensor: bfloat16 [4096, 1024], P('sp', 'tp'), may hold values from -6 to 6
- broad_emission_valve: bfloat16 [4096, 1024], P('sp', 'tp'), may hold values from -6 to 6
- slim_probe_tensor: bfloat16 [4096, 1024], P('sp', 'tp'), may hold values from -6 to 6
- slim_lookup_tensor: bfloat16 [4096, 1024], P('sp', 'tp'), may hold values from -6 to 6
- slim_payload_tensor: bfloat16 [4096, 1024], P('sp', 'tp'), may hold values from -6 to 6
- slim_emission_valve: bfloat16 [4096, 1024], P('sp', 'tp'), may hold values from -6 to 6
- broad_forgetting_speed: float32 [8], P('tp'), may hold values from -0.08 to 0
- slim_forgetting_speed: float32 [16], P('tp'), may hold values from -0.08 to 0
- broad_channel_scaling: float32 [1024], P('tp'), may hold values from 0.1 to 1.9
- slim_channel_scaling: float32 [1024], P('tp'), may hold values from 0.1 to 1.9
- surge_forgetting: float32 [4096], P('sp'), may hold values from -2.1 to 0
- broad_emission_proj: bfloat16 [1024, 2048], replicated, may hold values from -0.125 to 0.125
- slim_emission_proj: bfloat16 [1024, 2048], replicated, may hold values from -0.125 to 0.125
- skip_stream: bfloat16 [4096, 2048], P(('sp', 'tp')), may hold values from -6 to 6
- premix_scaling_coeffs: float32 [2048], replicated, may hold values from 0.1 to 1.9
- routed_specialist_ids: int32 [4096, 2], P('sp'), may hold values from 0 to 7, as said below
- routed_specialist_shares: float32 [4096, 2], P('sp'), may hold values from 0.2 to 1
- specialist_valve_proj: bfloat16 [8, 2048, 2048], P('sp', None, 'tp'), may hold values from -0.125 to 0.125
- specialist_expand_proj: bfloat16 [8, 2048, 2048], P('sp', None, 'tp'), may hold values from -0.125 to 0.125
- specialist_contract_proj: bfloat16 [8, 2048, 2048], P('sp', 'tp'), may hold values from -0.125 to 0.125
Outputs:
- result: bfloat16 [4096, 2048], P(('sp', 'tp'))
Inputs may be any that keep to these rules, and one draw needn't show every extreme that they name: `routed_specialist_ids`: each row names two different experts of one group, that is of the same run of 2 consecutive experts. The rows of one device (each aligned block of 128 rows) name each expert at most 64 times, and some expert is named exactly 64 times by the rows of every device.
All inputs are finite; a program needn't handle non-finite values.
Results may differ from a plain program's by a relative error of at most 0.018.
Values may be sent and summed in bfloat16 or wider, within the bound.
A program may use at most 128 MiB of HBM per device.

v0:
```python
import jax
import jax.numpy as jnp
from jax import lax
from jax.sharding import PartitionSpec as P

BROAD_CHANNEL_DIM = 128
THIN_CHANNEL_DIM = 64
GROUPS = 4


rope_base = 10000.0
epsilon = 1e-06


def entering(value, axis, join, neutral):
    place = lax.axis_index(axis)
    gathered = jax.tree.map(
        lambda a, kind: lax.all_gather(a.astype(kind), axis),
        value,
        (jnp.bfloat16, jnp.bfloat16, jnp.bfloat16, jnp.bfloat16),
    )
    state = jax.tree.map(lambda a, e: jnp.zeros_like(a) + jnp.asarray(e, a.dtype), value, neutral)

    def one(lap, state):
        return join(
            state,
            jax.tree.map(
                lambda a, own: lax.dynamic_index_in_dim(a, lap, 0, False).astype(own.dtype),
                gathered,
                value,
            ),
        )

    return lax.fori_loop(0, place, one, state)


def rotate(payload_tensor, positions):
    channel_dimension = payload_tensor.shape[-1]
    half = channel_dimension // 2
    freq = rope_base ** (-jnp.arange(half, dtype=jnp.float32) * 2.0 / channel_dimension)
    angle = positions.astype(jnp.float32)[:, None, None] * freq[None, None, :]
    cosine = jnp.cos(angle)
    sine = jnp.sin(angle)
    first = payload_tensor[..., :half]
    second = payload_tensor[..., half:]
    return jnp.concatenate([first * cosine - second * sine, first * sine + second * cosine], -1)


def segment_terms(probe_tensor, lookup_tensor, payload_tensor, surge_forgetting, forgetting_speed):
    length = probe_tensor.shape[0]
    segment_tally = jnp.arange(length, dtype=jnp.float32)
    memory_matrix = (
        forgetting_speed[None, :] * segment_tally[:, None] + jnp.cumsum(surge_forgetting)[:, None]
    )
    causal = (segment_tally[:, None] >= segment_tally[None, :])[None]
    level_t = jnp.transpose(memory_matrix)
    gap = level_t[:, :, None] - level_t[:, None, :]
    decay = jnp.where(causal, jnp.exp(jnp.where(causal, gap, 0.0)), 0.0)
    attention_scores = jnp.einsum(
        "szr,yzr->zsy", probe_tensor, lookup_tensor, preferred_element_type=jnp.float32
    )
    weights = (attention_scores * decay).astype(jnp.bfloat16)
    inner = jnp.einsum("htm,mhe->the", weights, payload_tensor, preferred_element_type=jnp.float32)
    factor = jnp.exp(memory_matrix + forgetting_speed[None, :])
    tail = jnp.exp(memory_matrix[-1:, :] - memory_matrix)
    weighted_output = (lookup_tensor.astype(jnp.float32) * tail[:, :, None]).astype(jnp.bfloat16)
    state_update = jnp.einsum(
        "oup,our->upr", weighted_output, payload_tensor, preferred_element_type=jnp.float32
    )
    total = jnp.exp(memory_matrix[-1] + forgetting_speed)
    return (inner, factor, state_update, total)


def read_state(probe_tensor, state):
    return jnp.einsum(
        "thd,hde->the", probe_tensor.astype(jnp.float32), state, precision=lax.Precision.HIGHEST
    )


def keeping_multiplier(
    probe_source,
    lookup_tensor,
    payload_tensor,
    forgetting_speed,
    surge_forgetting,
    channel_dimension,
    segment_begin,
):
    length = probe_source.shape[0]
    heads = probe_source.shape[1] // channel_dimension
    places = segment_begin + jnp.arange(length, dtype=jnp.int32)
    spun_probe = rotate(
        probe_source.astype(jnp.float32).reshape(length, heads, channel_dimension), places
    ).astype(jnp.bfloat16)
    spun_lookup = (
        rotate(lookup_tensor.astype(jnp.float32).reshape(length, heads, channel_dimension), places)
        * channel_dimension ** (-0.5)
    ).astype(jnp.bfloat16)
    regrouped_payload = payload_tensor.reshape(length, heads, channel_dimension)
    block = min(512, length)
    count = length // block

    def divider_mark(array):
        return array.reshape((count, block) + array.shape[1:])

    def segment_walker(carry, piece):
        state, prefix = carry
        block_q, block_k, block_v, block_b = piece
        inner, factor, state_update, total = segment_terms(
            block_q, block_k, block_v, block_b, forgetting_speed
        )
        local = inner + factor[:, :, None] * read_state(block_q, state)
        return (
            (total[:, None, None] * state + state_update, prefix * total),
            (local, factor * prefix[None, :]),
        )

    opening_location = (
        jnp.zeros((heads, channel_dimension, channel_dimension), jnp.float32),
        jnp.ones((heads,), jnp.float32),
    )
    (state, decay), (local, reach) = lax.scan(
        segment_walker,
        opening_location,
        (
            divider_mark(spun_probe),
            divider_mark(spun_lookup),
            divider_mark(regrouped_payload),
            divider_mark(surge_forgetting),
        ),
    )
    return (
        spun_probe,
        local.reshape(length, heads, channel_dimension),
        reach.reshape(length, heads),
        decay,
        state,
    )


def finish(sublayer_final, emission_valve, scaling_coefficients):
    length, heads, channel_dimension = sublayer_final.shape
    normed = sublayer_final * lax.rsqrt(
        jnp.mean(sublayer_final * sublayer_final, -1, keepdims=True) + epsilon
    )
    gated = (
        normed.reshape(length, heads * channel_dimension)
        * scaling_coefficients[None, :]
        * jax.nn.silu(emission_valve.astype(jnp.float32))
    )
    return gated.astype(jnp.bfloat16)


def chain(earlier, later):
    return (
        earlier[0] * later[0],
        later[0][:, None, None] * earlier[1] + later[1],
        earlier[2] * later[2],
        later[2][:, None, None] * earlier[3] + later[3],
    )


def slot_positions(chosen, experts, cap):
    listed = chosen.reshape(-1)
    matches = (listed[:, None] == jnp.arange(experts, dtype=jnp.int32)[None, :]).astype(jnp.int32)
    before = jnp.cumsum(matches, 0) - matches
    order = jnp.sum(before * matches, 1)
    return (listed * cap + order).reshape(chosen.shape)


def fill_slots(rows_in, chosen, experts, cap):
    count = rows_in.shape[0]
    places = slot_positions(chosen, experts, cap).reshape(-1)
    owners = jnp.repeat(jnp.arange(count, dtype=jnp.int32), 2)
    source = jnp.full((experts * cap,), count, jnp.int32).at[places].set(owners)
    padded = jnp.concatenate([rows_in, jnp.zeros((1, rows_in.shape[1]), rows_in.dtype)], 0)
    return padded[source].reshape(experts, cap, rows_in.shape[1])


def on_device(
    broad_probe_tensor,
    broad_lookup_tensor,
    broad_payload_tensor,
    broad_emission_valve,
    slim_probe_tensor,
    slim_lookup_tensor,
    slim_payload_tensor,
    slim_emission_valve,
    broad_forgetting_speed,
    slim_forgetting_speed,
    broad_channel_scaling,
    slim_channel_scaling,
    surge_forgetting,
    broad_emission_proj,
    slim_emission_proj,
    skip_stream,
    premix_scaling_coeffs,
    routed_specialist_ids,
    routed_specialist_shares,
    specialist_valve_proj,
    specialist_expand_proj,
    specialist_contract_proj,
):
    length = broad_probe_tensor.shape[0]
    segment_begin = lax.axis_index("sp") * length
    wide_result = keeping_multiplier(
        broad_probe_tensor,
        broad_lookup_tensor,
        broad_payload_tensor,
        broad_forgetting_speed,
        surge_forgetting,
        BROAD_CHANNEL_DIM,
        segment_begin,
    )
    narrow_result = keeping_multiplier(
        slim_probe_tensor,
        slim_lookup_tensor,
        slim_payload_tensor,
        slim_forgetting_speed,
        surge_forgetting,
        THIN_CHANNEL_DIM,
        segment_begin,
    )
    identity = (
        jnp.ones_like(wide_result[3]),
        jnp.zeros_like(wide_result[4]),
        jnp.ones_like(narrow_result[3]),
        jnp.zeros_like(narrow_result[4]),
    )
    incoming = entering(
        (wide_result[3], wide_result[4], narrow_result[3], narrow_result[4]), "sp", chain, identity
    )
    mixed_wide = finish(
        wide_result[1] + wide_result[2][:, :, None] * read_state(wide_result[0], incoming[1]),
        broad_emission_valve,
        broad_channel_scaling,
    )
    mixed_narrow = finish(
        narrow_result[1] + narrow_result[2][:, :, None] * read_state(narrow_result[0], incoming[3]),
        slim_emission_valve,
        slim_channel_scaling,
    )
    rows_wide, rows_narrow = (
        lax.all_to_all(mixed_wide, "tp", split_axis=0, concat_axis=1, tiled=True),
        lax.all_to_all(mixed_narrow, "tp", split_axis=0, concat_axis=1, tiled=True),
    )
    projected = jnp.dot(rows_wide, broad_emission_proj, preferred_element_type=jnp.float32)
    projected = projected + jnp.dot(
        rows_narrow, slim_emission_proj, preferred_element_type=jnp.float32
    )
    updated = skip_stream.astype(jnp.float32) + projected
    scale = lax.rsqrt(jnp.mean(updated * updated, -1, keepdims=True) + epsilon)
    normed = (updated * scale * premix_scaling_coeffs[None, :]).astype(jnp.bfloat16)
    rows = normed.shape[0]
    width = normed.shape[1]
    experts = lax.axis_size("sp") * specialist_valve_proj.shape[0]
    cap = rows * GROUPS // experts
    own_ids = lax.dynamic_slice_in_dim(routed_specialist_ids, lax.axis_index("tp") * rows, rows, 0)
    own_weights = lax.dynamic_slice_in_dim(
        routed_specialist_shares, lax.axis_index("tp") * rows, rows, 0
    )
    own_places = slot_positions(own_ids, experts, cap)
    sent = lax.all_to_all(
        fill_slots(normed, own_ids, experts, cap), "sp", split_axis=0, concat_axis=0, tiled=True
    )
    arrived = lax.all_gather(sent, "tp", axis=0, tiled=True)
    slots = arrived.reshape(-1, width)
    emission_valve = jnp.dot(slots, specialist_valve_proj[0], preferred_element_type=jnp.float32)
    up = jnp.dot(slots, specialist_expand_proj[0], preferred_element_type=jnp.float32)
    hidden = (jax.nn.silu(emission_valve) * up).astype(jnp.bfloat16)
    summed = lax.psum_scatter(
        jnp.dot(hidden, specialist_contract_proj[0], preferred_element_type=jnp.float32).astype(
            jnp.bfloat16
        ),
        "tp",
        scatter_dimension=0,
        tiled=True,
    )
    expert_out = summed.reshape(experts, cap, width)
    returned = lax.all_to_all(expert_out, "sp", split_axis=0, concat_axis=0, tiled=True)
    picked = returned.reshape(experts * cap, width)[own_places]
    mixture = jnp.sum(own_weights[:, :, None] * picked.astype(jnp.float32), 1)
    return (updated + mixture).astype(jnp.bfloat16)


def solution(mesh):
    return jax.shard_map(
        on_device,
        mesh=mesh,
        in_specs=(
            P("sp", "tp"),
            P("sp", "tp"),
            P("sp", "tp"),
            P("sp", "tp"),
            P("sp", "tp"),
            P("sp", "tp"),
            P("sp", "tp"),
            P("sp", "tp"),
            P("tp"),
            P("tp"),
            P("tp"),
            P("tp"),
            P("sp"),
            P(),
            P(),
            P(("sp", "tp"), None),
            P(),
            P("sp", None),
            P("sp", None),
            P("sp", None, "tp"),
            P("sp", None, "tp"),
            P("sp", "tp", None),
        ),
        out_specs=P(("sp", "tp"), None),
        check_vma=False,
    )
```

profile of v0, /device:TPU:0, one launch (start us, length us, event | category | flops | bytes accessed | tf_op | source)
XLA Modules:
  0.0 457.7 jit_solution(8412599231634419023)
XLA Ops:
  11.2 1.3 add_exponential_fusion
  22.6 1.7 subtract_convert_fusion
  25.0 35.2 %all-gather.1 = bf16[16,128,128]{2,1,0:T(8,128)(2,1)} all-gather(bf16[2,128,128]{2,1,0:T(8,128)(2,1)S(1)} %fusion.21), channel_id=3, replica_groups=mesh['sp'=8,'tp'=4] {'sp'}, dimensions={0}, use_global_device_ids=true | all-gather | bytes 589824 | tf_op jit(solution)/shard_map/all_gather | solution.py:18
  61.4 1.9 copy.154
  63.3 1.8 copy.150
  68.0 1.8 subtract_convert_fusion.1
  71.8 31.2 %all-gather.3 = bf16[32,64,64]{2,1,0:T(8,128)(2,1)S(1)} all-gather(bf16[4,64,64]{2,1,0:T(8,128)(2,1)S(1)} %fusion.22), channel_id=5, replica_groups=mesh['sp'=8,'tp'=4] {'sp'}, dimensions={0}, use_global_device_ids=true | all-gather | bytes 294912 | tf_op jit(solution)/shard_map/all_gather | solution.py:18
  103.0 21.7 %all-reduce.3 = (bf16[16]{0:T(256)(128)(2,1)S(1)}, bf16[32]{0:T(256)(128)(2,1)S(1)}) all-reduce(bf16[16]{0:T(256)(128)(2,1)} %copy-done.18, bf16[32]{0:T(256)(128)(2,1)} %copy-done.17), channel_id=2, replica_groups=mesh['sp'=8,'tp'=4] {'sp'}, use_global_device_ids=true, to_apply=%add.1 | all-reduce | flops 48 | bytes 192
  126.1 1.3 fusion.20
  127.4 4.2 fusion.12
  131.6 1.5 multiply_reduce_fusion.2
  135.2 1.6 fusion.37
  136.8 3.6 all-to-all-start.1
  142.2 3.1 fusion.11
  145.8 1.6 multiply_reduce_fusion.3
  149.1 1.4 scatter_custom_fusion
  150.5 1.8 fusion.38
  152.3 3.4 all-to-all-start
  156.0 5.7 %all-to-all-done = bf16[4,128,256]{2,1,0:T(8,128)(2,1)S(1)} async-done(((bf16[4,128,256]{2,1,0:T(8,128)(2,1)}), bf16[4,128,256]{2,1,0:T(8,128)(2,1)S(1)}, u32[]{:S(2)}, u32[]{:S(2)}) %all-to-all-start) | async-done | bytes 262176 | tf_op jit(solution)/shard_map/all_to_all | solution.py:244
  161.9 3.1 fusion.73
  167.5 3.3 gather_fusion
  170.8 66.0 %all_to_all.48 = bf16[8,64,2048]{2,1,0:T(8,128)(2,1)} all-to-all(bf16[8,64,2048]{2,1,0:T(8,128)(2,1)} %bitcast.121), channel_id=1, replica_groups=mesh['sp'=8,'tp'=4] {'sp'}, dimensions={0} | all-to-all | bytes 4194304 | tf_op jit(solution)/shard_map/all_to_all | solution.py:263
  237.2 56.4 %all-gather.6.cloned.1.call-done = bf16[32,64,2048]{2,1,0:T(8,128)(2,1)} async-done(((bf16[8,64,2048]{2,1,0:T(8,128)(2,1)}), bf16[32,64,2048]{2,1,0:T(8,128)(2,1)}) %all-gather.6.cloned.1.call-update) | async-done | bytes 8388624 | tf_op jit(solution)/shard_map/all_gather | solution.py:266
  293.5 7.7 %fusion.7 = f32[2048,512]{1,0:T(8,128)S(1)} fusion(bf16[2048,2048]{1,0:T(8,128)(2,1)} %bitcast.140, bf16[1,2048,512]{2,1,0:T(8,128)(2,1)} %param.43), kind=kOutput, calls=%fused_computation.18 | convolution fusion | flops 4294967296 | bytes 14680064 | tf_op jit(solution)/shard_map/dot_general | solution.py:268
  301.2 5.2 %multiply_convert_fusion = bf16[2048,512]{1,0:T(8,128)(2,1)S(1)} fusion(f32[2048,512]{1,0:T(8,128)S(1)} %fusion.7, bf16[2048,2048]{1,0:T(8,128)(2,1)S(1)} %bitcast.141, bf16[1,2048,512]{2,1,0:T(8,128)(2,1)S(1)} %copy-done.14), kind=kOutput, calls=%fused_computation.12 | convolution fusion | flops 4301258752 | bytes 16777216 | tf_op jit(solution)/shard_map/dot_general | solution.py:269
  306.4 6.7 %convolution_convert_fusion = bf16[2048,2048]{1,0:T(8,128)(2,1)} fusion(bf16[2048,512]{1,0:T(8,128)(2,1)S(1)} %multiply_convert_fusion, bf16[1,512,2048]{2,1,0:T(8,128)(2,1)S(1)} %copy-done), kind=kOutput, calls=%fused_computation.11 | convolution fusion | flops 4299161600 | bytes 12582912 | tf_op jit(solution)/shard_map/dot_general | solution.py:272
  313.2 71.5 %reduce-scatter.2.cloned.1.call-done = bf16[512,2048]{1,0:T(8,128)(2,1)} async-done(((bf16[2048,2048]{1,0:T(8,128)(2,1)}), bf16[512,2048]{1,0:T(8,128)(2,1)}) %reduce-scatter.2.cloned.1.call-update) | async-done | bytes 2097168 | tf_op jit(solution)/shard_map/reduce_scatter | solution.py:271
  384.7 5.5 %all-to-all-start.3 = ((bf16[8,64,2048]{2,1,0:T(8,128)(2,1)}), bf16[8,64,2048]{2,1,0:T(8,128)(2,1)}, u32[]{:S(2)}, u32[]{:S(2)}) async-start(bf16[8,64,2048]{2,1,0:T(8,128)(2,1)} %bitcast.124), calls=%async_computation.4 | async-start | bytes 4194304 | tf_op jit(solution)/shard_map/all_to_all | solution.py:280
  391.2 47.2 %all-to-all-done.3 = bf16[8,64,2048]{2,1,0:T(8,128)(2,1)} async-done(((bf16[8,64,2048]{2,1,0:T(8,128)(2,1)}), bf16[8,64,2048]{2,1,0:T(8,128)(2,1)}, u32[]{:S(2)}, u32[]{:S(2)}) %all-to-all-start.3) | async-done | bytes 2097184 | tf_op jit(solution)/shard_map/all_to_all | solution.py:280
  438.4 4.2 gather_fusion.1
  442.7 2.4 reshape.736
  445.0 4.9 %multiply_reduce_fusion = f32[128,2048]{1,0:T(8,128)S(1)} fusion(f32[128,2,2048]{2,1,0:T(2,128)} %reshape.736, f32[128,2]{1,0:T(8,128)S(1)} %copy.159), kind=kLoop, calls=%fused_computation.20 | loop fusion | flops 786432 | bytes 3146752 | tf_op jit(solution)/shard_map/reduce_sum | solution.py:282
  (121 shorter events, 32.5 us)
Async XLA Ops:
  6.5 299.9 %copy-start = (bf16[1,512,2048]{2,1,0:T(8,128)(2,1)S(1)}, bf16[1,512,2048]{2,1,0:T(8,128)(2,1)}, u32[]{:S(2)}) copy-start(bf16[1,512,2048]{2,1,0:T(8,128)(2,1)} %param.45) | copy-start | bytes 6291460
  22.6 2.0 copy-start.15
  24.3 37.0 %copy-start.6 = (bf16[512,256]{1,0:T(8,128)(2,1)S(1)}, bf16[512,256]{1,0:T(8,128)(2,1)}, u32[]{:S(2)}) copy-start(bf16[512,256]{1,0:T(8,128)(2,1)} %param.29) | copy-start | bytes 786436
  24.5 35.8 %copy-start.8 = (bf16[512,2,128]{2,0,1:T(8,128)(2,1)}, bf16[512,2,128]{2,0,1:T(8,128)(2,1)S(1)}, u32[]{:S(2)}) copy-start(bf16[512,2,128]{2,0,1:T(8,128)(2,1)S(1)} %fusion.35) | copy-start | bytes 786436
  24.5 40.6 %copy-start.16 = (u32[32]{0:T(128)S(1)}, u32[32]{0:T(128)}, u32[]{:S(2)}) copy-start(u32[32]{0:T(128)} %constant.143) | copy-start | bytes 388
  67.2 0.5 copy-start.17
  67.4 0.6 copy-start.18
  69.9 0.7 copy-start.9
  69.9 1.9 copy-start.10
  127.4 4.2 copy-start.4
  133.1 2.1 copy-start.7
  136.8 15.5 %all-to-all-start.1 = ((bf16[4,128,256]{2,1,0:T(8,128)(2,1)}), bf16[4,128,256]{2,1,0:T(8,128)(2,1)S(1)}, u32[]{:S(2)}, u32[]{:S(2)}) async-start(bf16[4,128,256]{2,1,0:T(8,128)(2,1)} %bitcast.28), calls=%async_computation.1 | async-start | bytes 524288 | tf_op jit(solution)/shard_map/all_to_all | solution.py:245
  145.7 4.7 %copy-start.12 = (f32[256]{0:T(256)S(1)}, f32[256]{0:T(256)}, u32[]{:S(2)}) copy-start(f32[256]{0:T(256)} %param.34) | copy-start | bytes 3076
  152.3 9.4 %all-to-all-start = ((bf16[4,128,256]{2,1,0:T(8,128)(2,1)}), bf16[4,128,256]{2,1,0:T(8,128)(2,1)S(1)}, u32[]{:S(2)}, u32[]{:S(2)}) async-start(bf16[4,128,256]{2,1,0:T(8,128)(2,1)} %bitcast.20), calls=%async_computation | async-start | bytes 524288 | tf_op jit(solution)/shard_map/all_to_all | solution.py:244
  155.7 137.8 %all-gather.6.cloned.1.call-start = ((), (), s32[]{:S(2)}) async-start(), calls=%async_computation.5 | async-start | bytes 10485760 | tf_op jit(solution)/shard_map/all_gather | solution.py:266
  161.9 3.5 copy-start.3
  161.9 3.6 copy-start.5
  165.4 1.8 copy-start.11
  166.3 1.0 copy-start.1
  236.9 147.8 %reduce-scatter.2.cloned.1.call-start = ((), (), s32[]{:S(2)}) async-start(), calls=%async_computation.6 | async-start | bytes 10485760 | tf_op jit(solution)/shard_map/reduce_scatter | solution.py:271
  293.5 7.7 %copy-start.13 = (bf16[32,64,2048]{2,1,0:T(8,128)(2,1)S(1)}, bf16[32,64,2048]{2,1,0:T(8,128)(2,1)}, u32[]{:S(2)}) copy-start(bf16[32,64,2048]{2,1,0:T(8,128)(2,1)} %all-gather.6.cloned.1.call-done) | copy-start | bytes 25165828
  293.5 7.7 %copy-start.14 = (bf16[1,2048,512]{2,1,0:T(8,128)(2,1)S(1)}, bf16[1,2048,512]{2,1,0:T(8,128)(2,1)}, u32[]{:S(2)}) copy-start(bf16[1,2048,512]{2,1,0:T(8,128)(2,1)} %param.44) | copy-start | bytes 6291460
  384.7 53.7 %all-to-all-start.3 = ((bf16[8,64,2048]{2,1,0:T(8,128)(2,1)}), bf16[8,64,2048]{2,1,0:T(8,128)(2,1)}, u32[]{:S(2)}, u32[]{:S(2)}) async-start(bf16[8,64,2048]{2,1,0:T(8,128)(2,1)} %bitcast.124), calls=%async_computation.4 | async-start | bytes 4194304 | tf_op jit(solution)/shard_map/all_to_all | solution.py:280
  445.0 4.9 %copy-start.2 = (f32[128,2048]{1,0:T(8,128)S(1)}, f32[128,2048]{1,0:T(8,128)}, u32[]{:S(2)}) copy-start(f32[128,2048]{1,0:T(8,128)} %copy-done.1) | copy-start | bytes 3145732
Sparse Core Ops, SparseCore 0:
  237.0 56.4 all-gather.5
  313.3 71.3 reduce-scatter.1
where the time goes:
time: 459 us; the launch traced here: 458 us
  waiting for transfers between devices  181 us (39%)
  blocking collectives  154 us (34%)
  matrix products  37.3 us (8%)
  local copies, waits for them, and re-layouts  30.9 us (7%)
  other arithmetic  26.4 us (6%)
  between operations  15.2 us (3%)
  starting transfers between devices  12.8 us (3%)
    reduce_scatter x1, waiting for transfers between devices, on_device(): lax.psum_scatter(jnp.dot(hidden, specialist_contract_proj[0], preferred_e...  71.5 us
    all_gather x2, blocking collectives, entering(): lax.all_gather(a.astype(kind), axis)  66.5 us
    all_to_all x1, blocking collectives, on_device(): lax.all_to_all(fill_slots(normed, own_ids, experts, cap), 'sp', split_axi...  66 us
    all_gather x1, waiting for transfers between devices, on_device(): arrived = lax.all_gather(sent, 'tp', axis=0, tiled=True)  56.4 us
    all_to_all x1, waiting for transfers between devices, on_device(): lax.all_to_all(expert_out, 'sp', split_axis=0, concat_axis=0, tiled=True)  47.2 us
    unnamed x1, blocking collectives  21.7 us
    unnamed x51, local copies, waits for them, and re-layouts  11.2 us
  transfers between devices with their start and end apart: 5, of which 4 were waited for; matrix products, arithmetic and copies ran while one was open for 3% of the time, Pallas kernels for 0%

commit v1 on v0

--- a/solution.py
+++ b/solution.py
@@ -1,7 +1,12 @@
 import jax
 import jax.numpy as jnp
 from jax import lax
+from jax.experimental import pallas as pl
+from jax.experimental.pallas import tpu as pltpu
 from jax.sharding import PartitionSpec as P
+
+MESH = pl.DeviceIdType.MESH
+VMEM_SPEC = pl.BlockSpec(memory_space=pltpu.VMEM)
 
 BROAD_CHANNEL_DIM = 128
 THIN_CHANNEL_DIM = 64
@@ -12,26 +17,182 @@
 epsilon = 1e-06
 
 
-def entering(value, axis, join, neutral):
-    place = lax.axis_index(axis)
-    gathered = jax.tree.map(
-        lambda a, kind: lax.all_gather(a.astype(kind), axis),
-        value,
-        (jnp.bfloat16, jnp.bfloat16, jnp.bfloat16, jnp.bfloat16),
-    )
-    state = jax.tree.map(lambda a, e: jnp.zeros_like(a) + jnp.asarray(e, a.dtype), value, neutral)
-
-    def one(lap, state):
-        return join(
-            state,
-            jax.tree.map(
-                lambda a, own: lax.dynamic_index_in_dim(a, lap, 0, False).astype(own.dtype),
-                gathered,
-                value,
-            ),
-        )
-
-    return lax.fori_loop(0, place, one, state)
+def exchange_kernel(state_ref, tile_ref, states_ref, tiles_ref, send_sem, recv_sem):
+    me = lax.axis_index("sp")
+    count = states_ref.shape[0]
+    barrier = pltpu.get_barrier_semaphore()
+    for step in range(1, count):
+        pl.semaphore_signal(
+            barrier, inc=1, device_id={"sp": lax.rem(me + step, count)}, device_id_type=MESH
+        )
+    pl.semaphore_wait(barrier, count - 1)
+    copies = []
+    for step in range(1, count):
+        for kind, (src, dst) in enumerate(((state_ref, states_ref), (tile_ref, tiles_ref))):
+            copy = pltpu.make_async_remote_copy(
+                src_ref=src,
+                dst_ref=dst.at[me],
+                send_sem=send_sem.at[kind, step],
+                recv_sem=recv_sem.at[kind, step],
+                device_id={"sp": lax.rem(me + step, count)},
+                device_id_type=MESH,
+            )
+            copy.start()
+            copies.append(copy)
+    states_ref[me] = state_ref[...]
+    tiles_ref[me] = tile_ref[...]
+    for copy in copies:
+        copy.wait()
+
+
+def exchange(state, tile):
+    count = lax.axis_size("sp")
+    return pl.pallas_call(
+        exchange_kernel,
+        out_shape=(
+            jax.ShapeDtypeStruct((count,) + state.shape, state.dtype),
+            jax.ShapeDtypeStruct((count,) + tile.shape, tile.dtype),
+        ),
+        in_specs=[VMEM_SPEC] * 2,
+        out_specs=(VMEM_SPEC, VMEM_SPEC),
+        scratch_shapes=[
+            pltpu.SemaphoreType.DMA((2, count)),
+            pltpu.SemaphoreType.DMA((2, count)),
+        ],
+        compiler_params=pltpu.CompilerParams(collective_id=0, has_side_effects=True),
+        name="state_exchange",
+    )(state, tile)
+
+
+def greet_group(groups, pair):
+    me = lax.axis_index("sp")
+    group = me // pair
+    member = lax.rem(me, pair)
+    barrier = pltpu.get_barrier_semaphore()
+    for step in range(1, groups):
+        pl.semaphore_signal(
+            barrier,
+            inc=1,
+            device_id={"sp": lax.rem(group + step, groups) * pair + member},
+            device_id_type=MESH,
+        )
+    pl.semaphore_signal(
+        barrier, inc=1, device_id={"sp": group * pair + 1 - member}, device_id_type=MESH
+    )
+    pl.semaphore_wait(barrier, groups)
+    return group, member
+
+
+def dispatch_kernel(rows_ref, out_ref, send_far, recv_far, send_near, recv_near):
+    groups = rows_ref.shape[0]
+    pair = out_ref.shape[0]
+    group, member = greet_group(groups, pair)
+    partner = group * pair + 1 - member
+    far = []
+    for step in range(1, groups):
+        target = lax.rem(group + step, groups)
+        copy = pltpu.make_async_remote_copy(
+            src_ref=rows_ref.at[target],
+            dst_ref=out_ref.at[member, group],
+            send_sem=send_far.at[step],
+            recv_sem=recv_far.at[step],
+            device_id={"sp": target * pair + member},
+            device_id_type=MESH,
+        )
+        copy.start()
+        far.append(copy)
+    near = []
+    for step in range(groups):
+        origin = lax.rem(group - step + groups, groups)
+        if step > 0:
+            far[step - 1].wait_recv()
+        copy = pltpu.make_async_remote_copy(
+            src_ref=rows_ref.at[group] if step == 0 else out_ref.at[member, origin],
+            dst_ref=out_ref.at[member, origin],
+            send_sem=send_near.at[step],
+            recv_sem=recv_near.at[step],
+            device_id={"sp": partner},
+            device_id_type=MESH,
+        )
+        copy.start()
+        near.append(copy)
+        if step == 0:
+            out_ref[member, group] = rows_ref[group]
+    for copy in far:
+        copy.wait_send()
+    for copy in near:
+        copy.wait()
+
+
+def dispatch(rows, pair):
+    groups = rows.shape[0]
+    return pl.pallas_call(
+        dispatch_kernel,
+        out_shape=jax.ShapeDtypeStruct((pair,) + rows.shape, rows.dtype),
+        in_specs=[VMEM_SPEC],
+        out_specs=VMEM_SPEC,
+        scratch_shapes=[pltpu.SemaphoreType.DMA((groups,))] * 4,
+        compiler_params=pltpu.CompilerParams(collective_id=1, has_side_effects=True),
+        name="row_dispatch",
+    )(rows)
+
+
+def collect_kernel(parts_ref, out_ref, landed, joined, send_near, recv_near, send_far, recv_far):
+    pair, groups = parts_ref.shape[:2]
+    group, member = greet_group(groups, pair)
+    partner = group * pair + 1 - member
+    order = list(range(1, groups)) + [0]
+    near = {}
+    for step in order:
+        target = lax.rem(group + step, groups)
+        near[step] = pltpu.make_async_remote_copy(
+            src_ref=parts_ref.at[1 - member, target],
+            dst_ref=landed.at[target],
+            send_sem=send_near.at[step],
+            recv_sem=recv_near.at[step],
+            device_id={"sp": partner},
+            device_id_type=MESH,
+        )
+        near[step].start()
+    far = []
+    for step in order:
+        target = lax.rem(group + step, groups)
+        near[step].wait_recv()
+        total = (
+            parts_ref[member, target].astype(jnp.float32) + landed[target].astype(jnp.float32)
+        ).astype(out_ref.dtype)
+        if step == 0:
+            out_ref[group] = total
+        else:
+            joined[target] = total
+            copy = pltpu.make_async_remote_copy(
+                src_ref=joined.at[target],
+                dst_ref=out_ref.at[group],
+                send_sem=send_far.at[step],
+                recv_sem=recv_far.at[step],
+                device_id={"sp": target * pair + member},
+                device_id_type=MESH,
+            )
+            copy.start()
+            far.append(copy)
+    for step in order:
+        near[step].wait_send()
+    for copy in far:
+        copy.wait()
+
+
+def collect(parts):
+    pair, groups = parts.shape[:2]
+    return pl.pallas_call(
+        collect_kernel,
+        out_shape=jax.ShapeDtypeStruct(parts.shape[1:], parts.dtype),
+        in_specs=[VMEM_SPEC],
+        out_specs=VMEM_SPEC,
+        scratch_shapes=[pltpu.VMEM(parts.shape[1:], parts.dtype)] * 2
+        + [pltpu.SemaphoreType.DMA((groups,))] * 4,
+        compiler_params=pltpu.CompilerParams(collective_id=2, has_side_effects=True),
+        name="row_collect",
+    )(parts)
 
 
 def rotate(payload_tensor, positions):
@@ -67,7 +228,7 @@
     state_update = jnp.einsum(
         "oup,our->upr", weighted_output, payload_tensor, preferred_element_type=jnp.float32
     )
-    total = jnp.exp(memory_matrix[-1] + forgetting_speed)
+    total = memory_matrix[-1] + forgetting_speed
     return (inner, factor, state_update, total)
 
 
@@ -103,37 +264,27 @@
     def divider_mark(array):
         return array.reshape((count, block) + array.shape[1:])
 
-    def segment_walker(carry, piece):
-        state, prefix = carry
-        block_q, block_k, block_v, block_b = piece
-        inner, factor, state_update, total = segment_terms(
-            block_q, block_k, block_v, block_b, forgetting_speed
-        )
-        local = inner + factor[:, :, None] * read_state(block_q, state)
-        return (
-            (total[:, None, None] * state + state_update, prefix * total),
-            (local, factor * prefix[None, :]),
-        )
-
-    opening_location = (
-        jnp.zeros((heads, channel_dimension, channel_dimension), jnp.float32),
-        jnp.ones((heads,), jnp.float32),
-    )
-    (state, decay), (local, reach) = lax.scan(
-        segment_walker,
-        opening_location,
-        (
-            divider_mark(spun_probe),
-            divider_mark(spun_lookup),
-            divider_mark(regrouped_payload),
-            divider_mark(surge_forgetting),
-        ),
-    )
+    state, level, local, reach = None, None, [], []
+    for piece in zip(
+        divider_mark(spun_probe),
+        divider_mark(spun_lookup),
+        divider_mark(regrouped_payload),
+        divider_mark(surge_forgetting),
+    ):
+        inner, factor, state_update, total = segment_terms(*piece, forgetting_speed)
+        if state is None:
+            state, level = state_update, total
+        else:
+            inner = inner + factor[:, :, None] * read_state(piece[0], state)
+            factor = factor * jnp.exp(level)[None, :]
+            state, level = jnp.exp(total)[:, None, None] * state + state_update, level + total
+        local.append(inner)
+        reach.append(factor)
     return (
         spun_probe,
-        local.reshape(length, heads, channel_dimension),
-        reach.reshape(length, heads),
-        decay,
+        jnp.concatenate(local, 0),
+        jnp.concatenate(reach, 0),
+        level,
         state,
     )
 
@@ -151,13 +302,14 @@
     return gated.astype(jnp.bfloat16)
 
 
-def chain(earlier, later):
-    return (
-        earlier[0] * later[0],
-        later[0][:, None, None] * earlier[1] + later[1],
-        earlier[2] * later[2],
-        later[2][:, None, None] * earlier[3] + later[3],
-    )
+def carried(states, levels):
+    place = lax.axis_index("sp")
+    count = states.shape[0]
+    index = jnp.arange(count, dtype=jnp.int32)
+    between = (index[None, :] > index[:, None]) & (index[None, :] < place)
+    reach = jnp.sum(jnp.where(between[:, :, None], levels[None, :, :], 0.0), 1)
+    weight = jnp.where((index < place)[:, None], jnp.exp(reach), 0.0)
+    return jnp.sum(weight[:, :, None, None] * states.astype(jnp.float32), 0)
 
 
 def slot_positions(chosen, experts, cap):
@@ -203,6 +355,9 @@
 ):
     length = broad_probe_tensor.shape[0]
     segment_begin = lax.axis_index("sp") * length
+    valve_all = lax.all_gather(specialist_valve_proj[0], "tp")
+    expand_all = lax.all_gather(specialist_expand_proj[0], "tp")
+    contract_all = lax.all_gather(specialist_contract_proj[0], "tp")
     wide_result = keeping_multiplier(
         broad_probe_tensor,
         broad_lookup_tensor,
@@ -221,22 +376,54 @@
         THIN_CHANNEL_DIM,
         segment_begin,
     )
-    identity = (
-        jnp.ones_like(wide_result[3]),
-        jnp.zeros_like(wide_result[4]),
-        jnp.ones_like(narrow_result[3]),
-        jnp.zeros_like(narrow_result[4]),
-    )
-    incoming = entering(
-        (wide_result[3], wide_result[4], narrow_result[3], narrow_result[4]), "sp", chain, identity
+    rows = skip_stream.shape[0]
+    width = skip_stream.shape[1]
+    experts = lax.axis_size("sp") * specialist_valve_proj.shape[0]
+    cap = rows * GROUPS // experts
+    pair = experts // GROUPS
+    own_ids = lax.dynamic_slice_in_dim(routed_specialist_ids, lax.axis_index("tp") * rows, rows, 0)
+    own_weights = lax.dynamic_slice_in_dim(
+        routed_specialist_shares, lax.axis_index("tp") * rows, rows, 0
+    )
+    levels = jnp.concatenate([wide_result[3], narrow_result[3]])
+    tile = levels
+    if pair == 2:
+        group_of = own_ids[:, 0] // pair
+        named = group_of[:, None] == jnp.arange(GROUPS, dtype=jnp.int32)[None, :]
+        rank = jnp.cumsum(named.astype(jnp.int32), 0) - 1
+        own_slot = group_of * cap + jnp.sum(jnp.where(named, rank, 0), 1)
+        holds = own_slot[None, :] == jnp.arange(GROUPS * cap, dtype=jnp.int32)[:, None]
+        member_ids = own_ids - group_of[:, None] * pair
+        slot_shares = []
+        for member in range(pair):
+            share = jnp.sum(jnp.where(member_ids == member, own_weights, 0.0), 1)
+            slot_shares.append(jnp.sum(jnp.where(holds, share[None, :], 0.0), 1))
+        tile = jnp.concatenate([levels] + slot_shares)
+    tile_size = -(-tile.shape[0] // 1024) * 1024
+    tile = jnp.pad(tile, (0, tile_size - tile.shape[0])).reshape(-1, 128)
+    packed = jnp.concatenate(
+        [wide_result[4].reshape(-1, 128), narrow_result[4].reshape(-1, 128)], 0
+    ).astype(jnp.bfloat16)
+    states, tiles = exchange(packed, tile)
+    count = states.shape[0]
+    tiles = tiles.reshape(count, -1)
+    wide_heads = wide_result[3].shape[0]
+    both_heads = levels.shape[0]
+    cut = wide_result[4].size // 128
+    incoming_wide = carried(
+        states[:, :cut].reshape((count,) + wide_result[4].shape), tiles[:, :wide_heads]
+    )
+    incoming_narrow = carried(
+        states[:, cut:].reshape((count,) + narrow_result[4].shape),
+        tiles[:, wide_heads:both_heads],
     )
     mixed_wide = finish(
-        wide_result[1] + wide_result[2][:, :, None] * read_state(wide_result[0], incoming[1]),
+        wide_result[1] + wide_result[2][:, :, None] * read_state(wide_result[0], incoming_wide),
         broad_emission_valve,
         broad_channel_scaling,
     )
     mixed_narrow = finish(
-        narrow_result[1] + narrow_result[2][:, :, None] * read_state(narrow_result[0], incoming[3]),
+        narrow_result[1] + narrow_result[2][:, :, None] * read_state(narrow_result[0], incoming_narrow),
         slim_emission_valve,
         slim_channel_scaling,
     )
@@ -251,35 +438,44 @@
     updated = skip_stream.astype(jnp.float32) + projected
     scale = lax.rsqrt(jnp.mean(updated * updated, -1, keepdims=True) + epsilon)
     normed = (updated * scale * premix_scaling_coeffs[None, :]).astype(jnp.bfloat16)
-    rows = normed.shape[0]
-    width = normed.shape[1]
-    experts = lax.axis_size("sp") * specialist_valve_proj.shape[0]
-    cap = rows * GROUPS // experts
-    own_ids = lax.dynamic_slice_in_dim(routed_specialist_ids, lax.axis_index("tp") * rows, rows, 0)
-    own_weights = lax.dynamic_slice_in_dim(
-        routed_specialist_shares, lax.axis_index("tp") * rows, rows, 0
-    )
-    own_places = slot_positions(own_ids, experts, cap)
-    sent = lax.all_to_all(
-        fill_slots(normed, own_ids, experts, cap), "sp", split_axis=0, concat_axis=0, tiled=True
-    )
-    arrived = lax.all_gather(sent, "tp", axis=0, tiled=True)
-    slots = arrived.reshape(-1, width)
-    emission_valve = jnp.dot(slots, specialist_valve_proj[0], preferred_element_type=jnp.float32)
-    up = jnp.dot(slots, specialist_expand_proj[0], preferred_element_type=jnp.float32)
-    hidden = (jax.nn.silu(emission_valve) * up).astype(jnp.bfloat16)
-    summed = lax.psum_scatter(
-        jnp.dot(hidden, specialist_contract_proj[0], preferred_element_type=jnp.float32).astype(
-            jnp.bfloat16
-        ),
-        "tp",
-        scatter_dimension=0,
-        tiled=True,
-    )
-    expert_out = summed.reshape(experts, cap, width)
-    returned = lax.all_to_all(expert_out, "sp", split_axis=0, concat_axis=0, tiled=True)
-    picked = returned.reshape(experts * cap, width)[own_places]
-    mixture = jnp.sum(own_weights[:, :, None] * picked.astype(jnp.float32), 1)
+    if pair == 2:
+        spread = holds.astype(jnp.bfloat16)
+        filled = jnp.dot(spread, normed, preferred_element_type=jnp.float32).astype(jnp.bfloat16)
+        slots = dispatch(filled.reshape(GROUPS, cap, width), pair).reshape(-1, width)
+    else:
+        own_places = slot_positions(own_ids, experts, cap)
+        slots = lax.all_to_all(
+            fill_slots(normed, own_ids, experts, cap), "sp", split_axis=0, concat_axis=0, tiled=True
+        ).reshape(-1, width)
+    expert_out = None
+    for part in range(lax.axis_size("tp")):
+        emission_valve = jnp.dot(slots, valve_all[part], preferred_element_type=jnp.float32)
+        up = jnp.dot(slots, expand_all[part], preferred_element_type=jnp.float32)
+        hidden = (jax.nn.silu(emission_valve) * up).astype(jnp.bfloat16)
+        term = jnp.dot(hidden, contract_all[part], preferred_element_type=jnp.float32)
+        expert_out = term if expert_out is None else expert_out + term
+    if pair == 2:
+        place = lax.axis_index("sp")
+        shares = tiles[:, both_heads : both_heads + pair * GROUPS * cap]
+        shares = shares.reshape(GROUPS, pair, pair, GROUPS, cap)
+        shares = lax.dynamic_index_in_dim(shares, place % pair, 2, False)
+        shares = lax.dynamic_index_in_dim(shares, place // pair, 2, False)
+        shares = jnp.transpose(shares, (1, 0, 2)).reshape(-1, 1)
+        parts = (expert_out * shares).astype(jnp.bfloat16)
+        returned = collect(parts.reshape(pair, GROUPS, cap, width)).reshape(-1, width)
+        mixture = lax.dot_general(
+            spread, returned, (((0,), (0,)), ((), ())), preferred_element_type=jnp.float32
+        )
+    else:
+        returned = lax.all_to_all(
+            expert_out.astype(jnp.bfloat16).reshape(experts, cap, width),
+            "sp",
+            split_axis=0,
+            concat_axis=0,
+            tiled=True,
+        )
+        picked = returned.reshape(experts * cap, width)[own_places]
+        mixture = jnp.sum(own_weights[:, :, None] * picked.astype(jnp.float32), 1)
     return (updated + mixture).astype(jnp.bfloat16)
 
 

time: 459 us -> 270 us (0.59)
  blocking collectives: 154 us -> 0 us
  waiting for transfers between devices: 181 us -> 65.2 us
  Pallas kernels: 0 us -> 101 us
  local copies, waits for them, and re-layouts: 30.9 us -> 9.94 us
  matrix products: 37.3 us -> 56.9 us
  other arithmetic: 26.4 us -> 15.4 us
  starting transfers between devices: 12.8 us -> 7.21 us
    pallas_call x0 -> x3, Pallas kernels: none -> 101 us  [the longest x1 42.8 us: dispatch(): pl.pallas_call(dispatch_kernel, out_shape=jax.ShapeDtypeStruct((pair,) +...]
    reduce_scatter x1 -> x0, waiting for transfers between devices: 71.5 us -> none  [on_device(): lax.psum_scatter(jnp.dot(hidden, specialist_contract_proj[0], preferred_e...]
    all_gather x2 -> x0, blocking collectives: 66.5 us -> none  [entering(): lax.all_gather(a.astype(kind), axis)]
    all_to_all x1 -> x0, blocking collectives: 66 us -> none  [on_device(): lax.all_to_all(fill_slots(normed, own_ids, experts, cap), 'sp', split_axi...]
    all_to_all x1 -> x0, waiting for transfers between devices: 47.2 us -> none  [on_device(): lax.all_to_all(expert_out, 'sp', split_axis=0, concat_axis=0, tiled=True)]
    dot_general x3 -> x10, matrix products: 19.6 us -> 47.9 us  [the longest x4 31 us: on_device(): jnp.dot(hidden, contract_all[part], preferred_element_type=jnp.float32)]
    unnamed x1 -> x0, blocking collectives: 21.7 us -> none
    gather x2 -> x0, local copies, waits for them, and re-layouts: 7.57 us -> none  [the longest x1 4.22 us: on_device(): picked = returned.reshape(experts * cap, width)[own_places]]
  transfers between devices with their start and end apart: 5 -> 5, of which waited for: 4 -> 3; matrix products, arithmetic and copies ran while one was open for 3% -> 17% of each run, Pallas kernels for 0% -> 24%
where the time goes in v1:
time: 270 us
  Pallas kernels  101 us (37%)
  waiting for transfers between devices  65.2 us (24%)
  matrix products  56.9 us (21%)
  other arithmetic  15.4 us (6%)
  between operations  13.7 us (5%)
  local copies, waits for them, and re-layouts  9.94 us (4%)
  starting transfers between devices  7.21 us (3%)
    all_gather x1, waiting for transfers between devices, on_device(): contract_all = lax.all_gather(specialist_contract_proj[0], 'tp')  54.4 us
    pallas_call x1, Pallas kernels, dispatch(): pl.pallas_call(dispatch_kernel, out_shape=jax.ShapeDtypeStruct((pair,) +...  42.8 us
    pallas_call x1, Pallas kernels, collect(): pl.pallas_call(collect_kernel, out_shape=jax.ShapeDtypeStruct(parts.shape...  37.2 us
    dot_general x4, matrix products, on_device(): jnp.dot(hidden, contract_all[part], preferred_element_type=jnp.float32)  31 us
    pallas_call x1, Pallas kernels, exchange(): pl.pallas_call(exchange_kernel, out_shape=(jax.ShapeDtypeStruct((count,)...  21.3 us
    dot_general x4, matrix products, on_device(): jnp.dot(slots, valve_all[part], preferred_element_type=jnp.float32)  13.1 us
  transfers between devices with their start and end apart: 5, of which 3 were waited for; matrix products, arithmetic and copies ran while one was open for 17% of the time, Pallas kernels for 24%

profile of v1, /device:TPU:0, one launch (start us, length us, event | category | flops | bytes accessed | tf_op | source)
XLA Modules:
  0.0 269.6 jit_solution(15794440631034213515)
XLA Ops:
  13.5 0.8 copy.161
  15.3 1.1 copy.166
  16.4 1.1 copy.160
  20.7 1.0 select_reduce_fusion.2
  22.6 1.3 fusion.72.tile_ref
  23.9 1.0 multiply_cosine_fusion
  26.8 21.3 %state_exchange.1 = (bf16[8,384,128]{2,1,0:T(8,128)(2,1)}, f32[8,8,128]{2,1,0:T(8,128)}) custom-call(bf16[384,128]{1,0:T(8,128)(2,1)} %pad_maximum_fusion.5.state_ref, f32[8,128]{1,0:T(8,128)} %fusion.72.tile_ref), custom_call_target="tpu_custom_call" | custom-call | tf_op jit(solution)/shard_map/state_exchange/pallas_call | solution.py:50
  49.4 1.4 multiply_reduce_fusion.1
  50.9 1.2 fusion.23
  53.0 0.9 fusion.59
  53.9 3.5 %all-to-all-start = ((bf16[4,128,256]{2,1,0:T(8,128)(2,1)}), bf16[4,128,256]{2,1,0:T(8,128)(2,1)S(1)}, u32[]{:S(2)}, u32[]{:S(2)}) async-start(bf16[4,128,256]{2,1,0:T(8,128)(2,1)} %bitcast.18), calls=%async_computation | async-start | bytes 524288 | tf_op jit(solution)/shard_map/all_to_all | solution.py:431
  58.1 1.0 multiply_reduce_fusion.3
  59.4 2.1 fusion.24
  62.4 0.9 fusion.58
  63.3 3.4 %all-to-all-done = bf16[4,128,256]{2,1,0:T(8,128)(2,1)S(1)} async-done(((bf16[4,128,256]{2,1,0:T(8,128)(2,1)}), bf16[4,128,256]{2,1,0:T(8,128)(2,1)S(1)}, u32[]{:S(2)}, u32[]{:S(2)}) %all-to-all-start) | async-done | bytes 262176 | tf_op jit(solution)/shard_map/all_to_all | solution.py:431
  66.6 3.6 %all-to-all-start.1 = ((bf16[4,128,256]{2,1,0:T(8,128)(2,1)}), bf16[4,128,256]{2,1,0:T(8,128)(2,1)S(1)}, u32[]{:S(2)}, u32[]{:S(2)}) async-start(bf16[4,128,256]{2,1,0:T(8,128)(2,1)} %bitcast.25), calls=%async_computation.1 | async-start | bytes 524288 | tf_op jit(solution)/shard_map/all_to_all | solution.py:432
  70.7 5.3 %all-to-all-done.1 = bf16[4,128,256]{2,1,0:T(8,128)(2,1)S(1)} async-done(((bf16[4,128,256]{2,1,0:T(8,128)(2,1)}), bf16[4,128,256]{2,1,0:T(8,128)(2,1)S(1)}, u32[]{:S(2)}, u32[]{:S(2)}) %all-to-all-start.1) | async-done | bytes 262176 | tf_op jit(solution)/shard_map/all_to_all | solution.py:432
  76.2 3.1 %fusion.96 = f32[128,2048]{1,0:T(8,128)S(1)} fusion(bf16[128,1024]{0,1:T(8,128)(2,1)S(1)} %bitcast.178, bf16[1024,2048]{1,0:T(8,128)(2,1)} %param.35), kind=kOutput, calls=%fused_computation.195 | convolution fusion | flops 536870912 | bytes 5505024 | tf_op jit(solution)/shard_map/dot_general | solution.py:434
  79.8 0.9 multiply_reduce_fusion
  80.7 1.5 convolution_convert_fusion
  82.2 42.8 %row_dispatch.1 = bf16[2,4,64,2048]{3,2,1,0:T(8,128)(2,1)} custom-call(bf16[4,64,2048]{2,1,0:T(8,128)(2,1)} %bitcast.168), custom_call_target="tpu_custom_call" | custom-call | tf_op jit(solution)/shard_map/row_dispatch/pallas_call | solution.py:129
  125.0 4.7 %fusion.3 = f32[512,512]{1,0:T(8,128)} fusion(bf16[512,2048]{1,0:T(8,128)(2,1)} %bitcast.158, bf16[4,2048,512]{2,1,0:T(8,128)(2,1)} %all-gather.4.cloned.1.call-done), kind=kOutput, calls=%fused_computation.11 | convolution fusion | flops 1073741824 | bytes 5242880 | tf_op jit(solution)/shard_map/dot_general | solution.py:452
  129.7 3.9 %fusion.6 = f32[512,512]{1,0:T(8,128)} fusion(bf16[512,2048]{1,0:T(8,128)(2,1)S(1)} %bitcast.159, bf16[4,2048,512]{2,1,0:T(8,128)(2,1)} %all-gather.4.cloned.1.call-done), kind=kOutput, calls=%fused_computation.17 | convolution fusion | flops 1073741824 | bytes 5242880 | tf_op jit(solution)/shard_map/dot_general | solution.py:452
  133.6 2.2 fusion.9
  135.8 2.2 fusion.12
  138.1 54.4 %all-gather.8.cloned.1.call-done = bf16[4,512,2048]{2,1,0:T(8,128)(2,1)} async-done(((bf16[1,512,2048]{2,1,0:T(8,128)(2,1)}), bf16[4,512,2048]{2,1,0:T(8,128)(2,1)}) %all-gather.8.cloned.1.call-update) | async-done | bytes 8388624 | tf_op jit(solution)/shard_map/all_gather | solution.py:360
  192.5 6.9 %fusion.10 = f32[512,2048]{1,0:T(8,128)} fusion(bf16[4,512,2048]{2,1,0:T(8,128)(2,1)} %all-gather.8.cloned.1.call-done, bf16[512,2048]{1,0:T(8,128)(2,1)S(1)} %bitcast.162, bf16[4,2048,512]{2,1,0:T(8,128)(2,1)} %all-gather.6.cloned.1.call-done, f32[512,512]{1,0:T(8,128)} %fusion.12), kind=kOutput, calls=%fused_computation.25 | convolution fusion | flops 2149056512 | bytes 11534336 | tf_op jit(solution)/shard_map/dot_general | solution.py:455
  199.4 7.0 %fusion.7 = f32[512,2048]{1,0:T(8,128)} fusion(bf16[4,512,2048]{2,1,0:T(8,128)(2,1)} %all-gather.8.cloned.1.call-done, bf16[512,2048]{1,0:T(8,128)(2,1)S(1)} %bitcast.163, bf16[4,2048,512]{2,1,0:T(8,128)(2,1)} %all-gather.6.cloned.1.call-done, f32[512,512]{1,0:T(8,128)} %fusion.9), kind=kOutput, calls=%fused_computation.19 | convolution fusion | flops 2149056512 | bytes 11534336 | tf_op jit(solution)/shard_map/dot_general | solution.py:455
  206.4 7.0 %fusion.4 = f32[512,2048]{1,0:T(8,128)} fusion(bf16[4,512,2048]{2,1,0:T(8,128)(2,1)} %all-gather.8.cloned.1.call-done, bf16[512,2048]{1,0:T(8,128)(2,1)S(1)} %bitcast.164, bf16[4,2048,512]{2,1,0:T(8,128)(2,1)} %all-gather.6.cloned.1.call-done, f32[512,512]{1,0:T(8,128)} %fusion.6), kind=kOutput, calls=%fused_computation.13 | convolution fusion | flops 2149056512 | bytes 11534336 | tf_op jit(solution)/shard_map/dot_general | solution.py:455
  213.3 10.1 %multiply_convert_fusion = bf16[512,2048]{1,0:T(8,128)(2,1)} fusion(f32[512,2048]{1,0:T(8,128)} %fusion.4, f32[512,2048]{1,0:T(8,128)} %fusion.10, f32[512,2048]{1,0:T(8,128)} %fusion.7, bf16[4,512,2048]{2,1,0:T(8,128)(2,1)} %all-gather.8.cloned.1.call-done, f32[512]{0:T(512)S(1)} %mul.532, bf16[512,2048]{1,0:T(8,128)(2,1)S(1)} %bitcast.165, ...), kind=kOutput, calls=%fused_computation | convolution fusion | flops 2154299392 | bytes 22022144 | tf_op jit(solution)/shard_map/dot_general | solution.py:455
  223.5 37.2 %row_collect.1 = bf16[4,64,2048]{2,1,0:T(8,128)(2,1)} custom-call(bf16[2,4,64,2048]{3,2,1,0:T(8,128)(2,1)} %bitcast.166), custom_call_target="tpu_custom_call" | custom-call | tf_op jit(solution)/shard_map/row_collect/pallas_call | solution.py:186
  260.7 2.4 fusion.1
  (146 shorter events, 18.7 us)
Async XLA Ops:
  6.5 19.1 %copy-start = (bf16[512,256]{1,0:T(8,128)(2,1)S(1)}, bf16[512,256]{1,0:T(8,128)(2,1)}, u32[]{:S(2)}) copy-start(bf16[512,256]{1,0:T(8,128)(2,1)} %param.24) | copy-start | bytes 786436
  6.5 118.4 %all-gather.4.cloned.1.call-start = ((), (), s32[]{:S(2)}) async-start(), calls=%async_computation.2 | async-start | bytes 10485760 | tf_op jit(solution)/shard_map/all_gather | solution.py:358
  7.3 1.6 copy-start.25
  7.3 2.2 copy-start.18
  7.3 3.0 %copy-start.20 = (f32[4]{0:T(128)S(1)}, f32[4]{0:T(128)}, u32[]{:S(2)}) copy-start(f32[4]{0:T(128)} %param.31) | copy-start | bytes 52
  7.3 5.9 %copy-start.12 = (bf16[512,256]{1,0:T(8,128)(2,1)S(1)}, bf16[512,256]{1,0:T(8,128)(2,1)}, u32[]{:S(2)}) copy-start(bf16[512,256]{1,0:T(8,128)(2,1)} %param.22) | copy-start | bytes 786436
  7.3 6.0 %copy-start.13 = (bf16[512,256]{1,0:T(8,128)(2,1)S(1)}, bf16[512,256]{1,0:T(8,128)(2,1)}, u32[]{:S(2)}) copy-start(bf16[512,256]{1,0:T(8,128)(2,1)} %param.23) | copy-start | bytes 786436
  7.3 130.8 %all-gather.6.cloned.1.call-start = ((), (), s32[]{:S(2)}) async-start(), calls=%async_computation.3 | async-start | bytes 10485760 | tf_op jit(solution)/shard_map/all_gather | solution.py:359
  8.1 5.4 %copy-start.14 = (bf16[512,256]{1,0:T(8,128)(2,1)S(1)}, bf16[512,256]{1,0:T(8,128)(2,1)}, u32[]{:S(2)}) copy-start(bf16[512,256]{1,0:T(8,128)(2,1)} %param.28) | copy-start | bytes 786436
  8.1 184.4 %all-gather.8.cloned.1.call-start = ((), (), s32[]{:S(2)}) async-start(), calls=%async_computation.4 | async-start | bytes 10485760 | tf_op jit(solution)/shard_map/all_gather | solution.py:360
  9.7 2.6 copy-start.29
  11.7 2.9 %copy-start.28 = (s32[128,2]{0,1:T(2,128)}, s32[128,2]{0,1:T(2,128)S(1)}, u32[]{:S(2)}) copy-start(s32[128,2]{0,1:T(2,128)S(1)} %constant_dynamic-slice_fusion.2) | copy-start | bytes 3076
  12.3 2.4 copy-start.24
  17.5 2.1 copy-start.15
  22.4 2.8 %copy-start.22 = (s32[128]{0:T(128)}, s32[128]{0:T(128)S(1)}, u32[]{:S(2)}) copy-start(s32[128]{0:T(128)S(1)} %multiply_add_fusion.6) | copy-start | bytes 1540
  52.0 1.0 copy-start.6
  52.0 1.0 copy-start.26
  53.9 5.4 %copy-start.21 = (f32[4]{0:T(128)S(1)}, f32[4]{0:T(128)}, u32[]{:S(2)}) copy-start(f32[4]{0:T(128)} %param.31) | copy-start | bytes 52
  53.9 5.5 %copy-start.5 = (bf16[512,4,32]{0,2,1:T(8,128)(2,1)S(1)}, bf16[512,4,32]{0,2,1:T(8,128)(2,1)}, u32[]{:S(2)}) copy-start(bf16[512,4,32]{0,2,1:T(8,128)(2,1)} %get-tuple-element.20) | copy-start | bytes 393220
  53.9 5.5 %copy-start.9 = (f32[512,4,32]{0,2,1:T(8,128)S(1)}, f32[512,4,32]{0,2,1:T(8,128)}, u32[]{:S(2)}) copy-start(f32[512,4,32]{0,2,1:T(8,128)} %copy-done.8) | copy-start | bytes 786436
  53.9 5.5 %copy-start.11 = (f32[512,4,32]{0,2,1:T(8,128)S(1)}, f32[512,4,32]{0,2,1:T(8,128)}, u32[]{:S(2)}) copy-start(f32[512,4,32]{0,2,1:T(8,128)} %copy-done.10) | copy-start | bytes 786436
  53.9 5.5 %copy-start.16 = (bf16[512,256]{0,1:T(8,128)(2,1)S(1)}, bf16[512,256]{0,1:T(8,128)(2,1)}, u32[]{:S(2)}) copy-start(bf16[512,256]{0,1:T(8,128)(2,1)} %copy.161) | copy-start | bytes 786436
  53.9 12.8 %all-to-all-start = ((bf16[4,128,256]{2,1,0:T(8,128)(2,1)}), bf16[4,128,256]{2,1,0:T(8,128)(2,1)S(1)}, u32[]{:S(2)}, u32[]{:S(2)}) async-start(bf16[4,128,256]{2,1,0:T(8,128)(2,1)} %bitcast.18), calls=%async_computation | async-start | bytes 524288 | tf_op jit(solution)/shard_map/all_to_all | solution.py:431
  61.4 1.0 copy-start.7
  61.5 0.9 copy-start.27
  66.6 9.4 %all-to-all-start.1 = ((bf16[4,128,256]{2,1,0:T(8,128)(2,1)}), bf16[4,128,256]{2,1,0:T(8,128)(2,1)S(1)}, u32[]{:S(2)}, u32[]{:S(2)}) async-start(bf16[4,128,256]{2,1,0:T(8,128)(2,1)} %bitcast.25), calls=%async_computation.1 | async-start | bytes 524288 | tf_op jit(solution)/shard_map/all_to_all | solution.py:432
  76.2 3.5 %copy-start.3 = (bf16[1024,2048]{1,0:T(8,128)(2,1)S(1)}, bf16[1024,2048]{1,0:T(8,128)(2,1)}, u32[]{:S(2)}) copy-start(bf16[1024,2048]{1,0:T(8,128)(2,1)} %param.36) | copy-start | bytes 12582916
  76.2 3.6 %copy-start.4 = (bf16[128,2048]{1,0:T(8,128)(2,1)S(1)}, bf16[128,2048]{1,0:T(8,128)(2,1)}, u32[]{:S(2)}) copy-start(bf16[128,2048]{1,0:T(8,128)(2,1)} %param.37) | copy-start | bytes 1572868
  79.8 0.9 copy-start.23
  124.9 4.7 %copy-start.2 = (bf16[2,4,64,2048]{3,2,1,0:T(8,128)(2,1)S(1)}, bf16[2,4,64,2048]{3,2,1,0:T(8,128)(2,1)}, u32[]{:S(2)}) copy-start(bf16[2,4,64,2048]{3,2,1,0:T(8,128)(2,1)} %row_dispatch.1) | copy-start | bytes 6291460
  125.0 8.6 %copy-start.31 = (bf16[4,2048,512]{2,1,0:T(8,128)(2,1)S(1)}, bf16[4,2048,512]{2,1,0:T(8,128)(2,1)}, u32[]{:S(2)}) copy-start(bf16[4,2048,512]{2,1,0:T(8,128)(2,1)} %all-gather.4.cloned.1.call-done) | copy-start | bytes 25165828
  223.5 39.6 %copy-start.1 = (bf16[512,256]{1,0:T(8,128)(2,1)S(1)}, bf16[512,256]{1,0:T(8,128)(2,1)}, u32[]{:S(2)}) copy-start(bf16[512,256]{1,0:T(8,128)(2,1)} %param.24) | copy-start | bytes 786436
  (5 other events, 3.8 us)
Sparse Core Ops, SparseCore 0:
  8.9 63.8 all-gather.3
  74.3 58.2 all-gather.5
  134.2 58.2 all-gather.7
